TPU v7x, 512 devices: a 8x2x16 block of a 8x16x16 slice. The times are simulated.
512 devices in a mesh: grp: 2 (over y), fs: 16 (over z), tp: 16 (over x, core).
Axes of the slice: x: 8, y: 2, z: 16, core: 2. Of those that a mesh axis runs over, the one named last changes fastest.
The devices are a block of a 8x16x16 slice.
Arguments:
- tokens: bfloat16 [4096, 2048], P(('grp', 'fs')), parts along dimension 0, may hold values from -12 to 12, as said below
- mix_heads: bfloat16 [4096, 2048], P(('grp', 'fs'), 'tp'), parts along dimension 0, may hold values from -6 to 6
- norm_first: float32 [2048], replicated, may hold values from 0.1 to 1.9
- gate_first: bfloat16 [2048, 5632], P('fs', 'tp'), may hold values from -0.125 to 0.125
- up_first: bfloat16 [2048, 5632], P('fs', 'tp'), may hold values from -0.125 to 0.125
- down_first: bfloat16 [5632, 2048], P('tp', 'fs'), may hold values from -0.078125 to 0.078125
- out_weight: bfloat16 [2048, 2048], P('tp', 'fs'), may hold values from -0.125 to 0.125
- norm_second: float32 [2048], replicated, may hold values from 0.1 to 1.9
- gate_second: bfloat16 [2048, 5632], P('fs', 'tp'), may hold values from -0.125 to 0.125
- up_second: bfloat16 [2048, 5632], P('fs', 'tp'), may hold values from -0.125 to 0.125
- down_second: bfloat16 [5632, 2048], P('tp', 'fs'), may hold values from -0.078125 to 0.078125
Outputs:
- layer_out: bfloat16 [4096, 2048], P(('grp', 'fs')), parts along dimension 0
There are 2 independent parts, one for each index of `grp`. A program takes and returns all parts, laid end to end along the dimension named above; an argument that names none is the same for every part. Nothing has to cross between parts.
Inputs may be any that keep to these rules, and one draw needn't show every extreme that they name: Each row of tokens carries a scale of its own.
All inputs are finite; a program needn't handle non-finite values.
Results may differ from a plain program's by a relative error of at most 0.014.
Values may be sent and summed in bfloat16 or wider, within the bound.
A program may use at most 64 MiB of HBM per device.

v0:
```python
import jax
import jax.numpy as jnp
from jax import lax
from jax.sharding import PartitionSpec as P

EPS = 0.1


def side_by_side(arrays, axis, dim, along):
    both = jnp.concatenate(arrays, axis=along)
    result, at, done = (lax.all_gather(both, axis, axis=dim, tiled=True), 0, [])
    for a in arrays:
        done.append(lax.slice_in_dim(result, at, at + a.shape[along], axis=along))
        at += a.shape[along]
    return tuple(done)


def laid_out(tiles, dim):
    lengths = list(tiles.shape[1:])
    lengths[dim] *= tiles.shape[0]
    return jnp.moveaxis(tiles, 0, dim).reshape(lengths)


def sent_to_all(array, axis):
    size = lax.axis_size(axis)
    return lax.all_to_all(
        jnp.broadcast_to(array[None], (size, *array.shape)), axis, 0, 0, tiled=True
    )


def gather_directly(array, axis, dim):
    return laid_out(sent_to_all(array, axis), dim)


def in_blocks(array, dim, size):
    before, after = (array.shape[:dim], array.shape[dim + 1 :])
    return jnp.moveaxis(array.reshape(*before, size, -1, *after), dim, 0)


def sum_at_owner(array, axis, dim):
    size = lax.axis_size(axis)
    tiles = lax.all_to_all(in_blocks(array, dim, size), axis, 0, 0, tiled=True)
    return jnp.sum(tiles.astype(jnp.float32), axis=0)


def norm_rows(row_block, gain_vector):
    widened = row_block.astype(jnp.float32)
    scaled = widened * lax.rsqrt(jnp.mean(widened * widened, axis=-1, keepdims=True) + EPS)
    return (scaled * gain_vector).astype(jnp.bfloat16)


def gate_values(normed, gate_weight, value_weight):
    pieces = side_by_side((gate_weight, value_weight), "fs", 0, 1)
    return (
        jnp.dot(normed, pieces[0], preferred_element_type=jnp.float32),
        jnp.dot(normed, pieces[1], preferred_element_type=jnp.float32),
    )


def half_branch(normed, gate_weight, value_weight, down_weight):
    gates, values = gate_values(normed, gate_weight, value_weight)
    hidden = (jax.nn.silu(gates) * values).astype(jnp.bfloat16)
    return 0.5 * jnp.dot(
        hidden, gather_directly(down_weight, "fs", 1), preferred_element_type=jnp.float32
    )


def share_sum(block_terms):
    return sum_at_owner(block_terms.astype(jnp.bfloat16), "tp", 0)


def join_rows(row_block):
    return lax.all_gather(row_block, "tp", axis=0, tiled=True)


def local(
    tokens,
    mix_heads,
    norm_first,
    gate_first,
    up_first,
    down_first,
    out_weight,
    norm_second,
    gate_second,
    up_second,
    down_second,
):
    normed_one = norm_rows(tokens, norm_first)
    first_terms = half_branch(normed_one, gate_first, up_first, down_first)
    heads_out = jnp.dot(
        mix_heads, gather_directly(out_weight, "fs", 1), preferred_element_type=jnp.float32
    )
    first_terms = first_terms + heads_out
    share_rows = tokens.shape[0] // lax.axis_size("tp")
    offset = lax.axis_index("tp") * share_rows
    own_rows = lax.dynamic_slice_in_dim(tokens, offset, share_rows, 0).astype(jnp.float32)
    resid_two = own_rows + share_sum(first_terms)
    normed_two = join_rows(norm_rows(resid_two, norm_second))
    second_terms = half_branch(normed_two, gate_second, up_second, down_second)
    finished = (resid_two + share_sum(second_terms)).astype(jnp.bfloat16)
    return join_rows(finished)


def solution(mesh):
    in_specs = (
        P(("grp", "fs"), None),
        P(("grp", "fs"), "tp"),
        P(),
        P("fs", "tp"),
        P("fs", "tp"),
        P("tp", "fs"),
        P("tp", "fs"),
        P(),
        P("fs", "tp"),
        P("fs", "tp"),
        P("tp", "fs"),
    )
    out_specs = P(("grp", "fs"), None)
    return jax.shard_map(local, mesh=mesh, in_specs=in_specs, out_specs=out_specs, check_vma=False)
```

profile of v0, /device:TPU:65, one launch (start us, length us, event | category | flops | bytes accessed | tf_op | source)
XLA Modules:
  0.0 398.9 jit_solution(9208464378308235055)
XLA Ops:
  6.6 2.2 broadcast_in_dim.6
  8.8 44.4 %all-to-all-start = ((bf16[16,352,128]{2,1,0:T(8,128)(2,1)}), bf16[16,352,128]{2,1,0:T(8,128)(2,1)S(1)}, u32[]{:S(2)}, u32[]{:S(2)}) async-start(bf16[16,352,128]{2,1,0:T(8,128)(2,1)} %broadcast_in_dim.6), calls=%async_computation | async-start | bytes 2883584 | tf_op jit(solution)/shard_map/all_to_all | solution.py:26
  54.1 68.0 %all-to-all-done = bf16[16,352,128]{2,1,0:T(8,128)(2,1)S(1)} async-done(((bf16[16,352,128]{2,1,0:T(8,128)(2,1)}), bf16[16,352,128]{2,1,0:T(8,128)(2,1)S(1)}, u32[]{:S(2)}, u32[]{:S(2)}) %all-to-all-start) | async-done | bytes 1441824 | tf_op jit(solution)/shard_map/all_to_all | solution.py:26
  122.1 0.9 broadcast_in_dim.7
  123.0 13.5 %all-to-all-start.1 = ((bf16[16,128,128]{1,2,0:T(8,128)(2,1)}), bf16[16,128,128]{1,2,0:T(8,128)(2,1)S(1)}, u32[]{:S(2)}, u32[]{:S(2)}) async-start(bf16[16,128,128]{1,2,0:T(8,128)(2,1)} %broadcast_in_dim.7), calls=%async_computation.1 | async-start | bytes 1048576 | tf_op jit(solution)/shard_map/all_to_all | solution.py:26
  136.8 48.7 %all-gather.3.cloned.1.call-done = bf16[2048,704]{0,1:T(8,128)(2,1)} async-done(((bf16[128,704]{0,1:T(8,128)(2,1)}), bf16[2048,704]{0,1:T(8,128)(2,1)}) %all-gather.3.cloned.1.call-update) | async-done | bytes 2883600 | tf_op jit(solution)/shard_map/all_gather | solution.py:11
  185.5 2.0 fusion.14
  187.5 3.1 convolution_multiply_fusion.1
  190.6 1.1 fusion.3
  191.7 15.7 %all-to-all-start.2 = ((bf16[16,8,2048]{2,1,0:T(8,128)(2,1)}), bf16[16,8,2048]{2,1,0:T(8,128)(2,1)S(1)}, u32[]{:S(2)}, u32[]{:S(2)}) async-start(bf16[16,8,2048]{2,1,0:T(8,128)(2,1)} %fusion.3), calls=%async_computation.2 | async-start | bytes 1048576 | tf_op jit(solution)/shard_map/all_to_all | solution.py:42
  207.5 0.7 pad_maximum_fusion.1
  208.3 16.4 %all-to-all-done.2 = bf16[16,8,2048]{2,1,0:T(8,128)(2,1)S(1)} async-done(((bf16[16,8,2048]{2,1,0:T(8,128)(2,1)}), bf16[16,8,2048]{2,1,0:T(8,128)(2,1)S(1)}, u32[]{:S(2)}, u32[]{:S(2)}) %all-to-all-start.2) | async-done | bytes 524320 | tf_op jit(solution)/shard_map/all_to_all | solution.py:42
  224.6 1.3 broadcast_in_dim.8
  225.9 8.3 %all-to-all-start.3 = ((bf16[16,352,128]{2,1,0:T(8,128)(2,1)}), bf16[16,352,128]{2,1,0:T(8,128)(2,1)S(1)}, u32[]{:S(2)}, u32[]{:S(2)}) async-start(bf16[16,352,128]{2,1,0:T(8,128)(2,1)} %broadcast_in_dim.8), calls=%async_computation.3 | async-start | bytes 2883584 | tf_op jit(solution)/shard_map/all_to_all | solution.py:26
  234.3 0.9 multiply_reduce_fusion
  235.2 0.8 multiply_convert_fusion
  236.0 16.0 %all_gather.13 = bf16[128,2048]{1,0:T(8,128)(2,1)S(1)} all-gather(bf16[8,2048]{1,0:T(8,128)(2,1)S(1)} %multiply_convert_fusion), channel_id=1, replica_groups=mesh['grp'=2,'fs'=16,'tp'=16] {'tp'}, dimensions={0}, use_global_device_ids=true | all-gather | bytes 557056 | tf_op jit(solution)/shard_map/all_gather | solution.py:73
  252.0 86.3 %all-gather.5.cloned.1.call-done = bf16[2048,704]{0,1:T(8,128)(2,1)} async-done(((bf16[128,704]{0,1:T(8,128)(2,1)}), bf16[2048,704]{0,1:T(8,128)(2,1)}) %all-gather.5.cloned.1.call-update) | async-done | bytes 2883600 | tf_op jit(solution)/shard_map/all_gather | solution.py:11
  338.3 1.9 fusion.10
  340.2 2.8 fusion.2
  343.1 31.3 %all_to_all.25 = bf16[16,8,2048]{2,1,0:T(8,128)(2,1)S(1)} all-to-all(bf16[16,8,2048]{2,1,0:T(8,128)(2,1)S(1)} %fusion.2), channel_id=1, replica_groups=mesh['grp'=2,'fs'=16,'tp'=16] {'tp'}, dimensions={0} | all-to-all | bytes 1048576 | tf_op jit(solution)/shard_map/all_to_all | solution.py:42
  374.5 0.8 add_convert_fusion
  375.2 16.0 %all_gather.15 = bf16[128,2048]{1,0:T(8,128)(2,1)S(1)} all-gather(bf16[8,2048]{1,0:T(8,128)(2,1)S(1)} %add_convert_fusion), channel_id=1, replica_groups=mesh['grp'=2,'fs'=16,'tp'=16] {'tp'}, dimensions={0}, use_global_device_ids=true | all-gather | bytes 557056 | tf_op jit(solution)/shard_map/all_gather | solution.py:73
  391.2 0.8 copy.27
  (33 shorter events, 1.4 us)
Async XLA Ops:
  6.5 184.0 %copy-start = (bf16[128,128]{1,0:T(8,128)(2,1)S(1)}, bf16[128,128]{1,0:T(8,128)(2,1)}, u32[]{:S(2)}) copy-start(bf16[128,128]{1,0:T(8,128)(2,1)} %param.12) | copy-start | bytes 98308
  8.8 44.5 %copy-start.2 = (bf16[128,352]{0,1:T(8,128)(2,1)S(1)}, bf16[128,352]{0,1:T(8,128)(2,1)}, u32[]{:S(2)}) copy-start(bf16[128,352]{0,1:T(8,128)(2,1)} %param.15) | copy-start | bytes 270340
  8.8 44.5 %copy-start.3 = (bf16[128,352]{0,1:T(8,128)(2,1)S(1)}, bf16[128,352]{0,1:T(8,128)(2,1)}, u32[]{:S(2)}) copy-start(bf16[128,352]{0,1:T(8,128)(2,1)} %param.14) | copy-start | bytes 270340
  8.8 45.2 %copy-start.7 = (bf16[128,128]{1,0:T(8,128)(2,1)S(1)}, bf16[128,128]{1,0:T(8,128)(2,1)}, u32[]{:S(2)}) copy-start(bf16[128,128]{1,0:T(8,128)(2,1)} %param.17) | copy-start | bytes 98308
  8.8 113.4 %all-to-all-start = ((bf16[16,352,128]{2,1,0:T(8,128)(2,1)}), bf16[16,352,128]{2,1,0:T(8,128)(2,1)S(1)}, u32[]{:S(2)}, u32[]{:S(2)}) async-start(bf16[16,352,128]{2,1,0:T(8,128)(2,1)} %broadcast_in_dim.6), calls=%async_computation | async-start | bytes 2883584 | tf_op jit(solution)/shard_map/all_to_all | solution.py:26
  53.1 83.4 %copy-start.1 = (bf16[128,2048]{1,0:T(8,128)(2,1)S(1)}, bf16[128,2048]{1,0:T(8,128)(2,1)}, u32[]{:S(2)}) copy-start(bf16[128,2048]{1,0:T(8,128)(2,1)} %param.11) | copy-start | bytes 1572868
  53.1 132.4 %copy-start.9 = (f32[2048]{0:T(1024)S(1)}, f32[2048]{0:T(1024)}, u32[]{:S(2)}) copy-start(f32[2048]{0:T(1024)} %param.13) | copy-start | bytes 24580
  53.1 132.3 %all-gather.3.cloned.1.call-start = ((), (), s32[]{:S(2)}) async-start(), calls=%async_computation.5 | async-start | bytes 3063808 | tf_op jit(solution)/shard_map/all_gather | solution.py:11
  123.0 67.6 %all-to-all-start.1 = ((bf16[16,128,128]{1,2,0:T(8,128)(2,1)}), bf16[16,128,128]{1,2,0:T(8,128)(2,1)S(1)}, u32[]{:S(2)}, u32[]{:S(2)}) async-start(bf16[16,128,128]{1,2,0:T(8,128)(2,1)} %broadcast_in_dim.7), calls=%async_computation.1 | async-start | bytes 1048576 | tf_op jit(solution)/shard_map/all_to_all | solution.py:26
  190.6 16.9 %copy-start.4 = (bf16[128,352]{0,1:T(8,128)(2,1)S(1)}, bf16[128,352]{0,1:T(8,128)(2,1)}, u32[]{:S(2)}) copy-start(bf16[128,352]{0,1:T(8,128)(2,1)} %param.20) | copy-start | bytes 270340
  190.6 16.9 %copy-start.5 = (bf16[128,352]{0,1:T(8,128)(2,1)S(1)}, bf16[128,352]{0,1:T(8,128)(2,1)}, u32[]{:S(2)}) copy-start(bf16[128,352]{0,1:T(8,128)(2,1)} %param.19) | copy-start | bytes 270340
  190.6 34.0 %copy-start.6 = (bf16[352,128]{1,0:T(8,128)(2,1)S(1)}, bf16[352,128]{1,0:T(8,128)(2,1)}, u32[]{:S(2)}) copy-start(bf16[352,128]{1,0:T(8,128)(2,1)} %param.21) | copy-start | bytes 270340
  191.7 32.9 %all-to-all-start.2 = ((bf16[16,8,2048]{2,1,0:T(8,128)(2,1)}), bf16[16,8,2048]{2,1,0:T(8,128)(2,1)S(1)}, u32[]{:S(2)}, u32[]{:S(2)}) async-start(bf16[16,8,2048]{2,1,0:T(8,128)(2,1)} %fusion.3), calls=%async_computation.2 | async-start | bytes 1048576 | tf_op jit(solution)/shard_map/all_to_all | solution.py:42
  207.4 130.9 %all-gather.5.cloned.1.call-start = ((), (), s32[]{:S(2)}) async-start(), calls=%async_computation.6 | async-start | bytes 3063808 | tf_op jit(solution)/shard_map/all_gather | solution.py:11
  225.9 9.3 %copy-start.8 = (f32[2048]{0:T(1024)S(1)}, f32[2048]{0:T(1024)}, u32[]{:S(2)}) copy-start(f32[2048]{0:T(1024)} %param.18) | copy-start | bytes 24580
  225.9 114.3 %all-to-all-start.3 = ((bf16[16,352,128]{2,1,0:T(8,128)(2,1)}), bf16[16,352,128]{2,1,0:T(8,128)(2,1)S(1)}, u32[]{:S(2)}, u32[]{:S(2)}) async-start(bf16[16,352,128]{2,1,0:T(8,128)(2,1)} %broadcast_in_dim.8), calls=%async_computation.3 | async-start | bytes 2883584 | tf_op jit(solution)/shard_map/all_to_all | solution.py:26
Sparse Core Ops, SparseCore 0:
  56.0 129.4 all-gather.2
  210.3 127.9 all-gather.4
where the time goes:
time: 400 us; the launch traced here: 399 us
  waiting for transfers between devices  220 us (55%)
  starting transfers between devices  82 us (20%)
  blocking collectives  63.3 us (16%)
  between operations  13.6 us (3%)
  matrix products  10.9 us (3%)
  local copies, waits for them, and re-layouts  5.35 us (1%)
  other arithmetic  4.25 us (1%)
    all_gather x2, waiting for transfers between devices, side_by_side(): result, at, done = (lax.all_gather(both, axis, axis=dim, tiled=True), 0, [])  135 us
    all_to_all x3, waiting for transfers between devices, sent_to_all(): lax.all_to_all(jnp.broadcast_to(array[None], (size, *array.shape)), axis,...  68 us
    all_to_all x3, starting transfers between devices, sent_to_all(): lax.all_to_all(jnp.broadcast_to(array[None], (size, *array.shape)), axis,...  66.1 us
    all_gather x2, blocking collectives, join_rows(): return lax.all_gather(row_block, 'tp', axis=0, tiled=True)  32 us
    all_to_all x1, blocking collectives, sum_at_owner(): tiles = lax.all_to_all(in_blocks(array, dim, size), axis, 0, 0, tiled=True)  31.3 us
    all_to_all x1, waiting for transfers between devices, sum_at_owner(): tiles = lax.all_to_all(in_blocks(array, dim, size), axis, 0, 0, tiled=True)  16.4 us
    all_to_all x1, starting transfers between devices, sum_at_owner(): tiles = lax.all_to_all(in_blocks(array, dim, size), axis, 0, 0, tiled=True)  15.7 us
  transfers between devices with their start and end apart: 6, of which 4 were waited for; matrix products, arithmetic and copies ran while one was open for 3% of the time, Pallas kernels for 0%

commit v1 on v0

--- a/solution.py
+++ b/solution.py
@@ -1,9 +1,31 @@
+import functools
 import jax
 import jax.numpy as jnp
 from jax import lax
 from jax.sharding import PartitionSpec as P
 
 EPS = 0.1
+
+
+def draft_the_inputs(x_in, mesh_name):
+    k_all = lax.axis_size(mesh_name)
+    cards = tuple(((k, (k + 1) % k_all) for k in range(k_all)))
+    vals = tuple(((k, (k - 1) % k_all) for k in range(k_all)))
+    side_arr, o_now = ([x_in], [x_in])
+    for _ in range(k_all // 2):
+        f_next = lax.ppermute(side_arr[-1], mesh_name, cards)
+        side_arr.append(f_next)
+    src_i = 0
+    while src_i < (k_all - 1) // 2:
+        state_now = lax.ppermute(o_now[-1], mesh_name, vals)
+        o_now.append(state_now)
+        src_i = src_i + 1
+    opened = jnp.concatenate([*side_arr[::-1], *o_now[1:]], axis=0)
+    arr_now = lax.axis_index(mesh_name)
+    return jnp.roll(opened, shift=(arr_now - k_all // 2) * x_in.shape[0], axis=0)
+
+
+frames_start = functools.partial(draft_the_inputs, mesh_name="tp")
 
 
 def side_by_side(arrays, axis, dim, along):
@@ -70,7 +92,7 @@
 
 
 def join_rows(row_block):
-    return lax.all_gather(row_block, "tp", axis=0, tiled=True)
+    return frames_start(row_block)
 
 
 def local(

time: 400 us -> 418 us (1.045)
  starting transfers between devices: 82 us -> 131 us
  blocking collectives: 63.3 us -> 31.1 us
    ppermute x0 -> x30, starting transfers between devices: none -> 48.9 us  [the longest x14 37.1 us: draft_the_inputs(): state_now = lax.ppermute(o_now[-1], mesh_name, vals)]
    all_gather x2 -> x0, blocking collectives: 32 us -> none  [join_rows(): return lax.all_gather(row_block, 'tp', axis=0, tiled=True)]
    all_gather x2, waiting for transfers between devices: 135 us -> 117 us  [side_by_side(): result, at, done = (lax.all_gather(both, axis, axis=dim, tiled=True), 0, [])]
    ppermute x0 -> x30, waiting for transfers between devices: none -> 16.2 us  [the longest x16 9.23 us: draft_the_inputs(): f_next = lax.ppermute(side_arr[-1], mesh_name, cards)]
  transfers between devices with their start and end apart: 6 -> 36, of which waited for: 4 -> 29; matrix products, arithmetic and copies ran while one was open for 3% -> 3% of each run, Pallas kernels for 0% -> 0%
where the time goes in v1:
time: 418 us; the launch traced here: 415 us
  waiting for transfers between devices  218 us (52%)
  starting transfers between devices  131 us (31%)
  blocking collectives  31.1 us (7%)
  between operations  13.9 us (3%)
  matrix products  11.1 us (3%)
  other arithmetic  5.35 us (1%)
  local copies, waits for them, and re-layouts  4.69 us (1%)
    all_gather x2, waiting for transfers between devices, side_by_side(): result, at, done = (lax.all_gather(both, axis, axis=dim, tiled=True), 0, [])  117 us
    all_to_all x3, waiting for transfers between devices, sent_to_all(): lax.all_to_all(jnp.broadcast_to(array[None], (size, *array.shape)), axis,...  68 us
    all_to_all x3, starting transfers between devices, sent_to_all(): lax.all_to_all(jnp.broadcast_to(array[None], (size, *array.shape)), axis,...  66.1 us
    ppermute x14, starting transfers between devices, draft_the_inputs(): state_now = lax.ppermute(o_now[-1], mesh_name, vals)  37.1 us
    all_to_all x1, blocking collectives, sum_at_owner(): tiles = lax.all_to_all(in_blocks(array, dim, size), axis, 0, 0, tiled=True)  31.1 us
    all_to_all x1, waiting for transfers between devices, sum_at_owner(): tiles = lax.all_to_all(in_blocks(array, dim, size), axis, 0, 0, tiled=True)  16.4 us
    all_to_all x1, starting transfers between devices, sum_at_owner(): tiles = lax.all_to_all(in_blocks(array, dim, size), axis, 0, 0, tiled=True)  15.7 us
    ppermute x16, starting transfers between devices, draft_the_inputs(): f_next = lax.ppermute(side_arr[-1], mesh_name, cards)  11.8 us
  transfers between devices with their start and end apart: 36, of which 29 were waited for; matrix products, arithmetic and copies ran while one was open for 3% of the time, Pallas kernels for 0%

profile of v1, /device:TPU:65, one launch (start us, length us, event | category | flops | bytes accessed | tf_op | source)
XLA Modules:
  0.0 414.9 jit_solution(5712282073954802865)
XLA Ops:
  6.6 2.2 broadcast_in_dim.6
  8.8 44.4 %all-to-all-start = ((bf16[16,352,128]{2,1,0:T(8,128)(2,1)}), bf16[16,352,128]{2,1,0:T(8,128)(2,1)S(1)}, u32[]{:S(2)}, u32[]{:S(2)}) async-start(bf16[16,352,128]{2,1,0:T(8,128)(2,1)} %broadcast_in_dim.6), calls=%async_computation | async-start | bytes 2883584 | tf_op jit(solution)/shard_map/all_to_all | solution.py:48
  54.1 68.0 %all-to-all-done = bf16[16,352,128]{2,1,0:T(8,128)(2,1)S(1)} async-done(((bf16[16,352,128]{2,1,0:T(8,128)(2,1)}), bf16[16,352,128]{2,1,0:T(8,128)(2,1)S(1)}, u32[]{:S(2)}, u32[]{:S(2)}) %all-to-all-start) | async-done | bytes 1441824 | tf_op jit(solution)/shard_map/all_to_all | solution.py:48
  123.0 13.5 %all-to-all-start.1 = ((bf16[16,128,128]{1,2,0:T(8,128)(2,1)}), bf16[16,128,128]{1,2,0:T(8,128)(2,1)S(1)}, u32[]{:S(2)}, u32[]{:S(2)}) async-start(bf16[16,128,128]{1,2,0:T(8,128)(2,1)} %broadcast_in_dim.7), calls=%async_computation.1 | async-start | bytes 1048576 | tf_op jit(solution)/shard_map/all_to_all | solution.py:48
  136.8 48.7 %all-gather.3.cloned.1.call-done = bf16[2048,704]{0,1:T(8,128)(2,1)} async-done(((bf16[128,704]{0,1:T(8,128)(2,1)}), bf16[2048,704]{0,1:T(8,128)(2,1)}) %all-gather.3.cloned.1.call-update) | async-done | bytes 2883600 | tf_op jit(solution)/shard_map/all_gather | solution.py:33
  187.5 3.1 convolution_multiply_fusion.1
  191.7 15.7 %all-to-all-start.2 = ((bf16[16,8,2048]{2,1,0:T(8,128)(2,1)}), bf16[16,8,2048]{2,1,0:T(8,128)(2,1)S(1)}, u32[]{:S(2)}, u32[]{:S(2)}) async-start(bf16[16,8,2048]{2,1,0:T(8,128)(2,1)} %fusion.3), calls=%async_computation.2 | async-start | bytes 1048576 | tf_op jit(solution)/shard_map/all_to_all | solution.py:64
  208.2 16.4 %all-to-all-done.2 = bf16[16,8,2048]{2,1,0:T(8,128)(2,1)S(1)} async-done(((bf16[16,8,2048]{2,1,0:T(8,128)(2,1)}), bf16[16,8,2048]{2,1,0:T(8,128)(2,1)S(1)}, u32[]{:S(2)}, u32[]{:S(2)}) %all-to-all-start.2) | async-done | bytes 524320 | tf_op jit(solution)/shard_map/all_to_all | solution.py:64
  225.9 8.3 %all-to-all-start.3 = ((bf16[16,352,128]{2,1,0:T(8,128)(2,1)}), bf16[16,352,128]{2,1,0:T(8,128)(2,1)S(1)}, u32[]{:S(2)}, u32[]{:S(2)}) async-start(bf16[16,352,128]{2,1,0:T(8,128)(2,1)} %broadcast_in_dim.8), calls=%async_computation.3 | async-start | bytes 2883584 | tf_op jit(solution)/shard_map/all_to_all | solution.py:48
  240.4 2.3 collective-permute-start.2
  246.9 2.3 collective-permute-start.10
  250.6 3.5 collective-permute-start.11
  255.0 4.1 collective-permute-start.12
  260.0 4.1 collective-permute-start.13
  264.9 4.1 collective-permute-start.14
  269.9 68.6 %all-gather.5.cloned.1.call-done = bf16[2048,704]{0,1:T(8,128)(2,1)} async-done(((bf16[128,704]{0,1:T(8,128)(2,1)}), bf16[2048,704]{0,1:T(8,128)(2,1)}) %all-gather.5.cloned.1.call-update) | async-done | bytes 2883600 | tf_op jit(solution)/shard_map/all_gather | solution.py:33
  340.5 2.9 fusion.2
  343.4 31.1 %all_to_all.25 = bf16[16,8,2048]{2,1,0:T(8,128)(2,1)S(1)} all-to-all(bf16[16,8,2048]{2,1,0:T(8,128)(2,1)S(1)} %fusion.2), channel_id=1, replica_groups=mesh['grp'=2,'fs'=16,'tp'=16] {'tp'}, dimensions={0} | all-to-all | bytes 1048576 | tf_op jit(solution)/shard_map/all_to_all | solution.py:64
  379.8 2.3 collective-permute-start.17
  385.7 2.2 collective-permute-start.25
  389.1 3.4 collective-permute-start.26
  393.3 3.7 collective-permute-start.27
  397.9 3.7 collective-permute-start.28
  402.4 3.7 collective-permute-start.29
  (123 shorter events, 38.9 us)
Async XLA Ops:
  8.8 113.4 %all-to-all-start = ((bf16[16,352,128]{2,1,0:T(8,128)(2,1)}), bf16[16,352,128]{2,1,0:T(8,128)(2,1)S(1)}, u32[]{:S(2)}, u32[]{:S(2)}) async-start(bf16[16,352,128]{2,1,0:T(8,128)(2,1)} %broadcast_in_dim.6), calls=%async_computation | async-start | bytes 2883584 | tf_op jit(solution)/shard_map/all_to_all | solution.py:48
  53.1 132.3 %all-gather.3.cloned.1.call-start = ((), (), s32[]{:S(2)}) async-start(), calls=%async_computation.5 | async-start | bytes 3063808 | tf_op jit(solution)/shard_map/all_gather | solution.py:33
  123.0 67.6 %all-to-all-start.1 = ((bf16[16,128,128]{1,2,0:T(8,128)(2,1)}), bf16[16,128,128]{1,2,0:T(8,128)(2,1)S(1)}, u32[]{:S(2)}, u32[]{:S(2)}) async-start(bf16[16,128,128]{1,2,0:T(8,128)(2,1)} %broadcast_in_dim.7), calls=%async_computation.1 | async-start | bytes 1048576 | tf_op jit(solution)/shard_map/all_to_all | solution.py:48
  191.7 32.9 %all-to-all-start.2 = ((bf16[16,8,2048]{2,1,0:T(8,128)(2,1)}), bf16[16,8,2048]{2,1,0:T(8,128)(2,1)S(1)}, u32[]{:S(2)}, u32[]{:S(2)}) async-start(bf16[16,8,2048]{2,1,0:T(8,128)(2,1)} %fusion.3), calls=%async_computation.2 | async-start | bytes 1048576 | tf_op jit(solution)/shard_map/all_to_all | solution.py:64
  207.4 131.0 %all-gather.5.cloned.1.call-start = ((), (), s32[]{:S(2)}) async-start(), calls=%async_computation.6 | async-start | bytes 3063808 | tf_op jit(solution)/shard_map/all_gather | solution.py:33
  225.9 114.6 %all-to-all-start.3 = ((bf16[16,352,128]{2,1,0:T(8,128)(2,1)}), bf16[16,352,128]{2,1,0:T(8,128)(2,1)S(1)}, u32[]{:S(2)}, u32[]{:S(2)}) async-start(bf16[16,352,128]{2,1,0:T(8,128)(2,1)} %broadcast_in_dim.8), calls=%async_computation.3 | async-start | bytes 2883584 | tf_op jit(solution)/shard_map/all_to_all | solution.py:48
  240.4 4.5 %collective-permute-start.2 = (bf16[8,2048]{1,0:T(8,128)(2,1)S(1)}, bf16[8,2048]{1,0:T(8,128)(2,1)S(1)}, u32[]{:S(2)}, u32[]{:S(2)}) collective-permute-start(bf16[8,2048]{1,0:T(8,128)(2,1)S(1)} %collective-permute-done.1), channel_id=1, source_target_pairs={{0,1},{1,2},{2,3},{3,4},{4,5},{5,6},{6,7},{7,8},{8,9},{9,10},{10,1... | collective-permute-start | bytes 98312 | tf_op jit(solution)/shard_map/ppermute | solution.py:16
  244.9 4.6 %collective-permute-start.3 = (bf16[8,2048]{1,0:T(8,128)(2,1)S(1)}, bf16[8,2048]{1,0:T(8,128)(2,1)S(1)}, u32[]{:S(2)}, u32[]{:S(2)}) collective-permute-start(bf16[8,2048]{1,0:T(8,128)(2,1)S(1)} %collective-permute-done.2), channel_id=1, source_target_pairs={{0,1},{1,2},{2,3},{3,4},{4,5},{5,6},{6,7},{7,8},{8,9},{9,10},{10,1... | collective-permute-start | bytes 98312 | tf_op jit(solution)/shard_map/ppermute | solution.py:16
  249.5 4.7 %collective-permute-start.4 = (bf16[8,2048]{1,0:T(8,128)(2,1)S(1)}, bf16[8,2048]{1,0:T(8,128)(2,1)S(1)}, u32[]{:S(2)}, u32[]{:S(2)}) collective-permute-start(bf16[8,2048]{1,0:T(8,128)(2,1)S(1)} %collective-permute-done.3), channel_id=1, source_target_pairs={{0,1},{1,2},{2,3},{3,4},{4,5},{5,6},{6,7},{7,8},{8,9},{9,10},{10,1... | collective-permute-start | bytes 98312 | tf_op jit(solution)/shard_map/ppermute | solution.py:16
  250.6 4.4 %collective-permute-start.11 = (bf16[8,2048]{1,0:T(8,128)(2,1)S(1)}, bf16[8,2048]{1,0:T(8,128)(2,1)S(1)}, u32[]{:S(2)}, u32[]{:S(2)}) collective-permute-start(bf16[8,2048]{1,0:T(8,128)(2,1)S(1)} %collective-permute-done.10), channel_id=1, source_target_pairs={{0,15},{1,0},{2,1},{3,2},{4,3},{5,4},{6,5},{7,6},{8,7},{9,8},{10,9... | collective-permute-start | bytes 98312 | tf_op jit(solution)/shard_map/ppermute | solution.py:20
  254.2 5.0 %collective-permute-start.5 = (bf16[8,2048]{1,0:T(8,128)(2,1)S(1)}, bf16[8,2048]{1,0:T(8,128)(2,1)S(1)}, u32[]{:S(2)}, u32[]{:S(2)}) collective-permute-start(bf16[8,2048]{1,0:T(8,128)(2,1)S(1)} %collective-permute-done.4), channel_id=1, source_target_pairs={{0,1},{1,2},{2,3},{3,4},{4,5},{5,6},{6,7},{7,8},{8,9},{9,10},{10,1... | collective-permute-start | bytes 98312 | tf_op jit(solution)/shard_map/ppermute | solution.py:16
  255.0 5.0 %collective-permute-start.12 = (bf16[8,2048]{1,0:T(8,128)(2,1)S(1)}, bf16[8,2048]{1,0:T(8,128)(2,1)S(1)}, u32[]{:S(2)}, u32[]{:S(2)}) collective-permute-start(bf16[8,2048]{1,0:T(8,128)(2,1)S(1)} %collective-permute-done.11), channel_id=1, source_target_pairs={{0,15},{1,0},{2,1},{3,2},{4,3},{5,4},{6,5},{7,6},{8,7},{9,8},{10,9... | collective-permute-start | bytes 98312 | tf_op jit(solution)/shard_map/ppermute | solution.py:20
  259.1 5.0 %collective-permute-start.6 = (bf16[8,2048]{1,0:T(8,128)(2,1)S(1)}, bf16[8,2048]{1,0:T(8,128)(2,1)S(1)}, u32[]{:S(2)}, u32[]{:S(2)}) collective-permute-start(bf16[8,2048]{1,0:T(8,128)(2,1)S(1)} %collective-permute-done.5), channel_id=1, source_target_pairs={{0,1},{1,2},{2,3},{3,4},{4,5},{5,6},{6,7},{7,8},{8,9},{9,10},{10,1... | collective-permute-start | bytes 98312 | tf_op jit(solution)/shard_map/ppermute | solution.py:16
  260.0 5.0 %collective-permute-start.13 = (bf16[8,2048]{1,0:T(8,128)(2,1)S(1)}, bf16[8,2048]{1,0:T(8,128)(2,1)S(1)}, u32[]{:S(2)}, u32[]{:S(2)}) collective-permute-start(bf16[8,2048]{1,0:T(8,128)(2,1)S(1)} %collective-permute-done.12), channel_id=1, source_target_pairs={{0,15},{1,0},{2,1},{3,2},{4,3},{5,4},{6,5},{7,6},{8,7},{9,8},{10,9... | collective-permute-start | bytes 98312 | tf_op jit(solution)/shard_map/ppermute | solution.py:20
  264.1 5.0 %collective-permute-start.7 = (bf16[8,2048]{1,0:T(8,128)(2,1)S(1)}, bf16[8,2048]{1,0:T(8,128)(2,1)S(1)}, u32[]{:S(2)}, u32[]{:S(2)}) collective-permute-start(bf16[8,2048]{1,0:T(8,128)(2,1)S(1)} %collective-permute-done.6), channel_id=1, source_target_pairs={{0,1},{1,2},{2,3},{3,4},{4,5},{5,6},{6,7},{7,8},{8,9},{9,10},{10,1... | collective-permute-start | bytes 98312 | tf_op jit(solution)/shard_map/ppermute | solution.py:16
  264.9 5.0 %collective-permute-start.14 = (bf16[8,2048]{1,0:T(8,128)(2,1)S(1)}, bf16[8,2048]{1,0:T(8,128)(2,1)S(1)}, u32[]{:S(2)}, u32[]{:S(2)}) collective-permute-start(bf16[8,2048]{1,0:T(8,128)(2,1)S(1)} %collective-permute-done.13), channel_id=1, source_target_pairs={{0,15},{1,0},{2,1},{3,2},{4,3},{5,4},{6,5},{7,6},{8,7},{9,8},{10,9... | collective-permute-start | bytes 98312 | tf_op jit(solution)/shard_map/ppermute | solution.py:20
  384.0 4.6 %collective-permute-start.18 = (bf16[8,2048]{1,0:T(8,128)(2,1)S(1)}, bf16[8,2048]{1,0:T(8,128)(2,1)S(1)}, u32[]{:S(2)}, u32[]{:S(2)}) collective-permute-start(bf16[8,2048]{1,0:T(8,128)(2,1)S(1)} %collective-permute-done.17), channel_id=1, source_target_pairs={{0,1},{1,2},{2,3},{3,4},{4,5},{5,6},{6,7},{7,8},{8,9},{9,10},{10,1... | collective-permute-start | bytes 98312 | tf_op jit(solution)/shard_map/ppermute | solution.py:16
  388.6 4.6 %collective-permute-start.19 = (bf16[8,2048]{1,0:T(8,128)(2,1)S(1)}, bf16[8,2048]{1,0:T(8,128)(2,1)S(1)}, u32[]{:S(2)}, u32[]{:S(2)}) collective-permute-start(bf16[8,2048]{1,0:T(8,128)(2,1)S(1)} %collective-permute-done.18), channel_id=1, source_target_pairs={{0,1},{1,2},{2,3},{3,4},{4,5},{5,6},{6,7},{7,8},{8,9},{9,10},{10,1... | collective-permute-start | bytes 98312 | tf_op jit(solution)/shard_map/ppermute | solution.py:16
  393.1 4.6 %collective-permute-start.20 = (bf16[8,2048]{1,0:T(8,128)(2,1)S(1)}, bf16[8,2048]{1,0:T(8,128)(2,1)S(1)}, u32[]{:S(2)}, u32[]{:S(2)}) collective-permute-start(bf16[8,2048]{1,0:T(8,128)(2,1)S(1)} %collective-permute-done.19), channel_id=1, source_target_pairs={{0,1},{1,2},{2,3},{3,4},{4,5},{5,6},{6,7},{7,8},{8,9},{9,10},{10,1... | collective-permute-start | bytes 98312 | tf_op jit(solution)/shard_map/ppermute | solution.py:16
  393.3 4.6 %collective-permute-start.27 = (bf16[8,2048]{1,0:T(8,128)(2,1)S(1)}, bf16[8,2048]{1,0:T(8,128)(2,1)S(1)}, u32[]{:S(2)}, u32[]{:S(2)}) collective-permute-start(bf16[8,2048]{1,0:T(8,128)(2,1)S(1)} %collective-permute-done.26), channel_id=1, source_target_pairs={{0,15},{1,0},{2,1},{3,2},{4,3},{5,4},{6,5},{7,6},{8,7},{9,8},{10,9... | collective-permute-start | bytes 98312 | tf_op jit(solution)/shard_map/ppermute | solution.py:20
  397.7 4.6 %collective-permute-start.21 = (bf16[8,2048]{1,0:T(8,128)(2,1)S(1)}, bf16[8,2048]{1,0:T(8,128)(2,1)S(1)}, u32[]{:S(2)}, u32[]{:S(2)}) collective-permute-start(bf16[8,2048]{1,0:T(8,128)(2,1)S(1)} %collective-permute-done.20), channel_id=1, source_target_pairs={{0,1},{1,2},{2,3},{3,4},{4,5},{5,6},{6,7},{7,8},{8,9},{9,10},{10,1... | collective-permute-start | bytes 98312 | tf_op jit(solution)/shard_map/ppermute | solution.py:16
  397.9 4.6 %collective-permute-start.28 = (bf16[8,2048]{1,0:T(8,128)(2,1)S(1)}, bf16[8,2048]{1,0:T(8,128)(2,1)S(1)}, u32[]{:S(2)}, u32[]{:S(2)}) collective-permute-start(bf16[8,2048]{1,0:T(8,128)(2,1)S(1)} %collective-permute-done.27), channel_id=1, source_target_pairs={{0,15},{1,0},{2,1},{3,2},{4,3},{5,4},{6,5},{7,6},{8,7},{9,8},{10,9... | collective-permute-start | bytes 98312 | tf_op jit(solution)/shard_map/ppermute | solution.py:20
  402.2 4.6 %collective-permute-start.22 = (bf16[8,2048]{1,0:T(8,128)(2,1)S(1)}, bf16[8,2048]{1,0:T(8,128)(2,1)S(1)}, u32[]{:S(2)}, u32[]{:S(2)}) collective-permute-start(bf16[8,2048]{1,0:T(8,128)(2,1)S(1)} %collective-permute-done.21), channel_id=1, source_target_pairs={{0,1},{1,2},{2,3},{3,4},{4,5},{5,6},{6,7},{7,8},{8,9},{9,10},{10,1... | collective-permute-start | bytes 98312 | tf_op jit(solution)/shard_map/ppermute | solution.py:16
  402.4 4.6 %collective-permute-start.29 = (bf16[8,2048]{1,0:T(8,128)(2,1)S(1)}, bf16[8,2048]{1,0:T(8,128)(2,1)S(1)}, u32[]{:S(2)}, u32[]{:S(2)}) collective-permute-start(bf16[8,2048]{1,0:T(8,128)(2,1)S(1)} %collective-permute-done.28), channel_id=1, source_target_pairs={{0,15},{1,0},{2,1},{3,2},{4,3},{5,4},{6,5},{7,6},{8,7},{9,8},{10,9... | collective-permute-start | bytes 98312 | tf_op jit(solution)/shard_map/ppermute | solution.py:20
  (22 other events, 649.9 us)
Sparse Core Ops, SparseCore 0:
  56.0 129.4 all-gather.2
  210.3 128.1 all-gather.4
